TPU v7x, 512 devices: a whole 4x4x16 slice. The times are simulated.
512 devices in a mesh: fs: 64 (over z, y), tp: 8 (over x, core).
Axes of the slice: x: 4, y: 4, z: 16, core: 2. Of those that a mesh axis runs over, the one named last changes fastest.
Arguments:
- tokens: bfloat16 [49152, 2048], P('fs'), may hold values from -6 to 6
- norm_gain: float32 [2048], replicated, may hold values from 0.1 to 1.9
- up_weight: float32 [2048, 8192], P('fs', 'tp'), may hold values from -0.125 to 0.125
- up_scale: float32 [8192], P('tp'), may hold values from 0.5 to 2
- down_weight: float32 [8192, 2048], P('tp', 'fs'), may hold values from -0.0625 to 0.0625
- down_scale: float32 [2048], P('fs'), may hold values from 0.5 to 2
Outputs:
- output: bfloat16 [49152, 2048], P('fs', 'tp')
All inputs are finite; a program needn't handle non-finite values.
Results may differ from a plain program's by a relative error of at most 0.015.
Values may be sent and summed in bfloat16 or wider, within the bound.
No kernel may reach another device: no remote copies, remote signals or barrier semaphores. Data moves between devices by JAX's collectives and lax.ppermute only.
A program may use at most 64 MiB of HBM per device.

v0:
```python
import jax
import jax.numpy as jnp
from jax import lax
from jax.sharding import Mesh
from jax.sharding import PartitionSpec as P

FS = ("fs_0", "fs_1")


epsilon = 1e-06


def gathered_by_axis(array, axes, dim):
    result = array
    for number in range(len(axes) - 1, -1, -1):
        result = lax.all_gather(result, axes[number], axis=dim, tiled=True)
    return result


def cut_along(array, dim, count):
    before, after = (array.shape[:dim], array.shape[dim + 1 :])
    return jnp.moveaxis(array.reshape(*before, count, -1, *after), dim, 0)


def summed_on_arrival(array, axis, dim):
    count = lax.axis_size(axis)
    tiles = lax.all_to_all(cut_along(array, dim, count), axis, 0, 0, tiled=True)
    return jnp.sum(tiles.astype(jnp.float32), axis=0)


def local(tokens, norm_gain, up_weight, up_scale, down_weight, down_scale):
    floats = tokens.astype(jnp.float32)
    inverse = lax.rsqrt(jnp.mean(floats * floats, axis=-1, keepdims=True) + epsilon)
    normed = (floats * inverse * norm_gain).astype(jnp.bfloat16)
    up_half = up_weight.astype(jnp.bfloat16)
    down_half = down_weight.astype(jnp.bfloat16)
    up_whole, down_whole, scale_whole = (
        gathered_by_axis(up_half, FS, 0),
        gathered_by_axis(down_half, FS, 1),
        gathered_by_axis(down_scale.astype(jnp.bfloat16), FS, 0).astype(down_scale.dtype),
    )
    up_pre = jnp.dot(normed, up_whole, preferred_element_type=jnp.float32)
    hidden = jnp.square(jax.nn.relu(up_pre * up_scale)).astype(jnp.bfloat16)
    partial_value = jnp.dot(hidden, down_whole, preferred_element_type=jnp.float32).astype(
        jnp.bfloat16
    )
    summed = summed_on_arrival(partial_value.astype(jnp.float32).astype(jnp.bfloat16), "tp", 1)
    own_width = summed.shape[1]
    own_scale = lax.dynamic_slice_in_dim(
        scale_whole, lax.axis_index("tp") * own_width, own_width, 0
    )
    return (summed * own_scale).astype(jnp.bfloat16)


def solution(mesh):
    split = Mesh(mesh.devices.reshape(16, 4, mesh.shape["tp"]), ("fs_0", "fs_1", "tp"))
    return jax.shard_map(
        local,
        mesh=split,
        in_specs=(P(FS, None), P(), P(FS, "tp"), P("tp"), P("tp", FS), P(FS)),
        out_specs=P(FS, "tp"),
        check_vma=False,
    )
```

profile of v0, /device:TPU:1, one launch (start us, length us, event | category | flops | bytes accessed | tf_op | source)
XLA Modules:
  0.0 246.8 jit_solution(16874398824401263367)
XLA Ops:
  6.5 0.0 copy-start
  6.5 0.0 copy-start.1
  6.5 0.0 copy-start.2
  6.5 0.0 all-gather.6.cloned.1.call-start
  6.5 1.1 convert_element_type.36
  7.6 11.4 %all_gather.20 = bf16[1024,128]{0,1:T(8,128)(2,1)} all-gather(bf16[1024,32]{0,1:T(8,128)(2,1)S(1)} %convert_element_type.36), channel_id=1, replica_groups=mesh['fs_0'=16,'fs_1'=4,'tp'=8] {'fs_1'}, dimensions={1}, use_global_device_ids=true | all-gather | bytes 327680 | tf_op jit(solution)/shard_map/all_gather | solution.py:16
  19.0 0.0 all-gather.6.cloned.1.call-update
  19.1 0.0 all-gather.4.cloned.1.call-start
  19.1 0.9 convert_element_type.34
  20.0 10.1 %all_gather.18 = bf16[128,1024]{1,0:T(8,128)(2,1)} all-gather(bf16[32,1024]{1,0:T(8,128)(2,1)S(1)} %convert_element_type.34), channel_id=1, replica_groups=mesh['fs_0'=16,'fs_1'=4,'tp'=8] {'fs_1'}, dimensions={0}, use_global_device_ids=true | all-gather | bytes 327680 | tf_op jit(solution)/shard_map/all_gather | solution.py:16
  30.1 0.0 all-gather.4.cloned.1.call-update
  30.2 2.6 %fusion = f32[768]{0:T(1024)S(1)} fusion(bf16[768,2048]{1,0:T(8,128)(2,1)} %param.6), kind=kLoop, calls=%fused_computation.2 | loop fusion | flops 4717824 | bytes 3148800 | tf_op jit(solution)/shard_map/reduce_sum | solution.py:33
  32.8 61.9 %all-gather.6.cloned.1.call-done = bf16[1024,2048]{0,1:T(8,128)(2,1)} async-done(((bf16[1024,128]{0,1:T(8,128)(2,1)}), bf16[1024,2048]{0,1:T(8,128)(2,1)}) %all-gather.6.cloned.1.call-update) | async-done | bytes 4194320 | tf_op jit(solution)/shard_map/all_gather | solution.py:16
  94.6 77.2 %all-gather.4.cloned.1.call-done = bf16[2048,1024]{1,0:T(8,128)(2,1)} async-done(((bf16[128,1024]{1,0:T(8,128)(2,1)}), bf16[2048,1024]{1,0:T(8,128)(2,1)}) %all-gather.4.cloned.1.call-update) | async-done | bytes 4194320 | tf_op jit(solution)/shard_map/all_gather | solution.py:16
  171.8 0.0 copy-done
  171.8 0.0 copy-done.1
  171.8 0.0 copy-done.2
  171.8 11.9 %convolution_convert_fusion = bf16[768,2048]{1,0:T(8,128)(2,1)} fusion(bf16[1024,2048]{0,1:T(8,128)(2,1)} %all-gather.6.cloned.1.call-done, bf16[2048,1024]{1,0:T(8,128)(2,1)} %all-gather.4.cloned.1.call-done, bf16[768,2048]{1,0:T(8,128)(2,1)S(1)} %copy-done, f32[2048]{0:T(1024)S(1)} %copy-done.1, f32[768]{0:T(1024)S(1)} %add_rsqrt_fusion, ...), kind=kOutput, calls=%fused_computation.6 | convolution fusion | flops 6453460992 | bytes 14695424 | tf_op jit(solution)/shard_map/dot_general | solution.py:44
  183.7 3.7 %copy.10 = bf16[96,8,8,256]{3,2,0,1:T(8,128)(2,1)} copy(bf16[96,8,8,256]{3,2,1,0:T(8,128)(2,1)} %bitcast.12) | data formatting | bytes 6291456 | tf_op jit(solution)/shard_map/reshape | solution.py:22
  187.5 0.0 copy-start.3
  187.5 13.8 %all-to-all-start = ((bf16[8,768,256]{2,1,0:T(8,128)(2,1)}), bf16[8,768,256]{2,1,0:T(8,128)(2,1)S(1)}, u32[]{:S(2)}, u32[]{:S(2)}) async-start(bf16[8,768,256]{2,1,0:T(8,128)(2,1)} %bitcast.11), calls=%async_computation | async-start | bytes 6291456 | tf_op jit(solution)/shard_map/all_to_all | solution.py:27
  201.3 0.0 copy-done.3
  201.3 1.3 dynamic-slice
  203.2 0.2 dynamic-update-slice
  203.5 9.0 %all-reduce = bf16[128]{0:T(256)(128)(2,1)S(1)} all-reduce(bf16[128]{0:T(256)(128)(2,1)S(1)} %dynamic-update-slice), channel_id=1, replica_groups=mesh['fs_0'=16,'fs_1'=4,'tp'=8] {'fs_1'}, use_global_device_ids=true, to_apply=%add | all-reduce | flops 128 | bytes 512
  212.5 23.2 %all-gather = bf16[16,1,128]{2,1,0:T(2,128)(2,1)S(1)} all-gather(bf16[1,1,128]{2,1,0:T(2,128)(2,1)S(1)} %bitcast.14), channel_id=1, replica_groups=mesh['fs_0'=16,'fs_1'=4,'tp'=8] {'fs_0'}, dimensions={0}, use_global_device_ids=true | all-gather | bytes 4352 | tf_op jit(solution)/shard_map/all_gather | solution.py:16
  235.7 0.1 dynamic_slice.3
  235.8 2.9 %all-to-all-done = bf16[8,768,256]{2,1,0:T(8,128)(2,1)S(1)} async-done(((bf16[8,768,256]{2,1,0:T(8,128)(2,1)}), bf16[8,768,256]{2,1,0:T(8,128)(2,1)S(1)}, u32[]{:S(2)}, u32[]{:S(2)}) %all-to-all-start) | async-done | bytes 3145760 | tf_op jit(solution)/shard_map/all_to_all | solution.py:27
  238.7 0.4 convert_reduce_fusion
  239.2 0.8 multiply_convert_fusion.1
  (4 shorter events, 0.0 us)
Async XLA Ops:
  6.5 165.3 %copy-start = (bf16[768,2048]{1,0:T(8,128)(2,1)S(1)}, bf16[768,2048]{1,0:T(8,128)(2,1)}, u32[]{:S(2)}) copy-start(bf16[768,2048]{1,0:T(8,128)(2,1)} %param.6) | copy-start | bytes 9437188
  6.5 165.3 %copy-start.1 = (f32[2048]{0:T(1024)S(1)}, f32[2048]{0:T(1024)}, u32[]{:S(2)}) copy-start(f32[2048]{0:T(1024)} %param.7) | copy-start | bytes 24580
  6.5 165.3 %copy-start.2 = (f32[1024]{0:T(1024)S(1)}, f32[1024]{0:T(1024)}, u32[]{:S(2)}) copy-start(f32[1024]{0:T(1024)} %param.9) | copy-start | bytes 12292
  6.5 88.1 %all-gather.6.cloned.1.call-start = ((), (), s32[]{:S(2)}) async-start(), calls=%async_computation.2 | async-start | bytes 4456448 | tf_op jit(solution)/shard_map/all_gather | solution.py:16
  19.1 152.7 %all-gather.4.cloned.1.call-start = ((), (), s32[]{:S(2)}) async-start(), calls=%async_computation.1 | async-start | bytes 4456448 | tf_op jit(solution)/shard_map/all_gather | solution.py:16
  187.5 13.8 %copy-start.3 = (f32[32]{0:T(128)S(1)}, f32[32]{0:T(128)}, u32[]{:S(2)}) copy-start(f32[32]{0:T(128)} %param.11) | copy-start | bytes 388
  187.5 51.2 %all-to-all-start = ((bf16[8,768,256]{2,1,0:T(8,128)(2,1)}), bf16[8,768,256]{2,1,0:T(8,128)(2,1)S(1)}, u32[]{:S(2)}, u32[]{:S(2)}) async-start(bf16[8,768,256]{2,1,0:T(8,128)(2,1)} %bitcast.11), calls=%async_computation | async-start | bytes 6291456 | tf_op jit(solution)/shard_map/all_to_all | solution.py:27
Sparse Core Ops, SparseCore 0:
  19.2 75.4 all-gather.5
  96.7 75.0 all-gather.3
where the time goes:
time: 250 us; the launch traced here: 247 us
  waiting for transfers between devices  142 us (57%)
  blocking collectives  53.8 us (22%)
  between operations  14.1 us (6%)
  starting transfers between devices  13.8 us (6%)
  matrix products  11.9 us (5%)
  other arithmetic  5.82 us (2%)
  local copies, waits for them, and re-layouts  5.35 us (2%)
    all_gather x2, waiting for transfers between devices, gathered_by_axis(): result = lax.all_gather(result, axes[number], axis=dim, tiled=True)  139 us
    all_gather x3, blocking collectives, gathered_by_axis(): result = lax.all_gather(result, axes[number], axis=dim, tiled=True)  44.7 us
    all_to_all x1, starting transfers between devices, summed_on_arrival(): tiles = lax.all_to_all(cut_along(array, dim, count), axis, 0, 0, tiled=True)  13.8 us
    dot_general x1, matrix products, local(): jnp.dot(hidden, down_whole, preferred_element_type=jnp.float32)  11.9 us
    unnamed x1, blocking collectives  9.03 us
  transfers between devices with their start and end apart: 3, of which 3 were waited for; matrix products, arithmetic and copies ran while one was open for 2% of the time, Pallas kernels for 0%

commit v1 on v0

v1 whole, which is shorter than its diff:
```python
import jax
import jax.numpy as jnp
from jax import lax
from jax.sharding import Mesh
from jax.sharding import PartitionSpec as P

FS = ("fs_0", "fs_1")


epsilon = 1e-06


def cut_along(array, dim, count):
    before, after = (array.shape[:dim], array.shape[dim + 1 :])
    return jnp.moveaxis(array.reshape(*before, count, -1, *after), dim, 0)


def summed_on_arrival(array, axis, dim):
    count = lax.axis_size(axis)
    tiles = lax.all_to_all(cut_along(array, dim, count), axis, 0, 0, tiled=True)
    return jnp.sum(tiles.astype(jnp.float32), axis=0)


def local(tokens, norm_gain, up_weight, up_scale, down_weight, down_scale):
    up_half = up_weight.astype(jnp.bfloat16)
    down_rows = (down_weight.T * down_scale[:, None]).astype(jnp.bfloat16)
    up_whole = lax.all_gather(up_half, FS, axis=0, tiled=True)
    down_whole = lax.all_gather(down_rows, FS, axis=0, tiled=True)
    floats = tokens.astype(jnp.float32)
    inverse = lax.rsqrt(jnp.mean(floats * floats, axis=-1, keepdims=True) + epsilon)
    normed = (floats * inverse * norm_gain).astype(jnp.bfloat16)
    up_pre = jnp.dot(normed, up_whole, preferred_element_type=jnp.float32)
    hidden = jnp.square(jax.nn.relu(up_pre * up_scale)).astype(jnp.bfloat16)
    hidden = lax.optimization_barrier(hidden)
    partial_value = lax.dot_general(
        hidden, down_whole, (((1,), (1,)), ((), ())), preferred_element_type=jnp.float32
    ).astype(jnp.bfloat16)
    return summed_on_arrival(partial_value, "tp", 1).astype(jnp.bfloat16)


def solution(mesh):
    split = Mesh(mesh.devices.reshape(16, 4, mesh.shape["tp"]), ("fs_0", "fs_1", "tp"))
    return jax.shard_map(
        local,
        mesh=split,
        in_specs=(P(FS, None), P(), P(FS, "tp"), P("tp"), P("tp", FS), P(FS)),
        out_specs=P(FS, "tp"),
        check_vma=False,
    )
```

time: 250 us -> 362 us (1.45)
  waiting for transfers between devices: 142 us -> 277 us
  starting transfers between devices: 13.8 us -> 0.04 us
  local copies, waits for them, and re-layouts: 5.35 us -> 0.22 us
    all_gather x2, waiting for transfers between devices: 139 us -> 277 us  [the longest x1 140 us: local(): up_whole = lax.all_gather(up_half, FS, axis=0, tiled=True)]
    all_to_all x0 -> x1, blocking collectives: none -> 51.1 us  [summed_on_arrival(): tiles = lax.all_to_all(cut_along(array, dim, count), axis, 0, 0, tiled=True)]
    all_gather x3 -> x0, blocking collectives: 44.7 us -> none  [gathered_by_axis(): result = lax.all_gather(result, axes[number], axis=dim, tiled=True)]
    all_to_all x1 -> x0, starting transfers between devices: 13.8 us -> none  [summed_on_arrival(): tiles = lax.all_to_all(cut_along(array, dim, count), axis, 0, 0, tiled=True)]
    unnamed x1 -> x0, blocking collectives: 9.03 us -> none
    dot_general x1 -> x2, matrix products: 11.9 us -> 13 us  [the longest x1 6.89 us: local(): up_pre = jnp.dot(normed, up_whole, preferred_element_type=jnp.float32)]
  transfers between devices with their start and end apart: 3 -> 2, of which waited for: 3 -> 2; matrix products, arithmetic and copies ran while one was open for 2% -> 3% of each run, Pallas kernels for 0% -> 0%
where the time goes in v1:
time: 362 us
  waiting for transfers between devices  277 us (77%)
  blocking collectives  51.1 us (14%)
  between operations  13.4 us (4%)
  matrix products  13 us (4%)
  other arithmetic  7.15 us (2%)
    all_gather x1, waiting for transfers between devices, local(): up_whole = lax.all_gather(up_half, FS, axis=0, tiled=True)  140 us
    all_gather x1, waiting for transfers between devices, local(): down_whole = lax.all_gather(down_rows, FS, axis=0, tiled=True)  137 us
    all_to_all x1, blocking collectives, summed_on_arrival(): tiles = lax.all_to_all(cut_along(array, dim, count), axis, 0, 0, tiled=True)  51.1 us
  transfers between devices with their start and end apart: 2, of which 2 were waited for; matrix products, arithmetic and copies ran while one was open for 3% of the time, Pallas kernels for 0%

profile of v1, /device:TPU:1, one launch (start us, length us, event | category | flops | bytes accessed | tf_op | source)
XLA Modules:
  0.0 362.0 jit_solution(8417288208690118681)
XLA Ops:
  6.5 0.0 copy-start
  6.5 0.0 copy-start.2
  6.5 0.0 copy-start.1
  6.5 0.0 all-gather.3.cloned.1.call-start
  6.5 1.7 convert_element_type.25
  8.2 0.0 all-gather.3.cloned.1.call-update
  8.3 0.0 all-gather.5.cloned.1.call-start
  8.3 1.6 fusion.9
  9.9 0.0 all-gather.5.cloned.1.call-update
  9.9 2.6 fusion
  12.5 140.0 %all-gather.3.cloned.1.call-done = bf16[2048,1024]{1,0:T(8,128)(2,1)} async-done(((bf16[32,1024]{1,0:T(8,128)(2,1)}), bf16[2048,1024]{1,0:T(8,128)(2,1)}) %all-gather.3.cloned.1.call-update) | async-done | bytes 4194320 | tf_op jit(solution)/shard_map/all_gather | solution.py:27
  152.5 0.0 copy-done
  152.5 0.0 copy-done.2
  152.5 0.0 copy-done.1
  152.6 6.9 %multiply_convert_fusion = bf16[768,1024]{1,0:T(8,128)(2,1)} fusion(bf16[2048,1024]{1,0:T(8,128)(2,1)} %all-gather.3.cloned.1.call-done, bf16[768,2048]{1,0:T(8,128)(2,1)S(1)} %copy-done, f32[2048]{0:T(1024)S(1)} %copy-done.1, f32[768]{0:T(1024)S(1)} %add_rsqrt_fusion, f32[1024]{0:T(1024)S(1)} %copy-done.2), kind=kOutput, calls=%fused_computation.8 | convolution fusion | flops 3230662656 | bytes 8928256 | tf_op jit(solution)/shard_map/dot_general | solution.py:32
  159.4 137.0 %all-gather.5.cloned.1.call-done = bf16[2048,1024]{1,0:T(8,128)(2,1)} async-done(((bf16[32,1024]{1,0:T(8,128)(2,1)}), bf16[2048,1024]{1,0:T(8,128)(2,1)}) %all-gather.5.cloned.1.call-update) | async-done | bytes 4194320 | tf_op jit(solution)/shard_map/all_gather | solution.py:28
  296.4 6.1 %convolution_convert_fusion = bf16[768,2048]{1,0:T(8,128)(2,1)S(1)} fusion(bf16[768,1024]{1,0:T(8,128)(2,1)} %multiply_convert_fusion, bf16[2048,1024]{1,0:T(8,128)(2,1)} %all-gather.5.cloned.1.call-done), kind=kOutput, calls=%fused_computation.5 | convolution fusion | flops 3222798336 | bytes 8912896 | tf_op jit(solution)/shard_map/dot_general | solution.py:35
  302.5 0.2 copy.10
  302.8 51.1 %all_to_all.5 = bf16[8,768,256]{2,1,0:T(8,128)(2,1)S(1)} all-to-all(bf16[8,768,256]{2,1,0:T(8,128)(2,1)S(1)} %bitcast.12), channel_id=1, replica_groups=mesh['fs_0'=16,'fs_1'=4,'tp'=8] {'tp'}, dimensions={0} | all-to-all | bytes 6291456 | tf_op jit(solution)/shard_map/all_to_all | solution.py:20
  353.9 1.3 reduce_sum.22
  (1 shorter events, 0.0 us)
Async XLA Ops:
  6.5 146.0 %copy-start = (bf16[768,2048]{1,0:T(8,128)(2,1)S(1)}, bf16[768,2048]{1,0:T(8,128)(2,1)}, u32[]{:S(2)}) copy-start(bf16[768,2048]{1,0:T(8,128)(2,1)} %param.6) | copy-start | bytes 9437188
  6.5 146.0 %copy-start.2 = (f32[1024]{0:T(1024)S(1)}, f32[1024]{0:T(1024)}, u32[]{:S(2)}) copy-start(f32[1024]{0:T(1024)} %param.9) | copy-start | bytes 12292
  6.5 146.0 %copy-start.1 = (f32[2048]{0:T(1024)S(1)}, f32[2048]{0:T(1024)}, u32[]{:S(2)}) copy-start(f32[2048]{0:T(1024)} %param.7) | copy-start | bytes 24580
  6.5 146.0 %all-gather.3.cloned.1.call-start = ((), (), s32[]{:S(2)}) async-start(), calls=%async_computation.1 | async-start | bytes 4259840 | tf_op jit(solution)/shard_map/all_gather | solution.py:27
  8.3 288.2 %all-gather.5.cloned.1.call-start = ((), (), s32[]{:S(2)}) async-start(), calls=%async_computation.2 | async-start | bytes 4259840 | tf_op jit(solution)/shard_map/all_gather | solution.py:28
Sparse Core Ops, SparseCore 0:
  10.3 142.2 all-gather.2
  155.5 140.8 all-gather.4

commit v2 on v1

v2 whole, which is shorter than its diff:
```python
import jax
import jax.numpy as jnp
from jax import lax
from jax.experimental import pallas as pl
from jax.experimental.pallas import tpu as pltpu
from jax.sharding import Mesh
from jax.sharding import PartitionSpec as P

FS = ("z", "y")
TP = ("x", "c")

epsilon = 1e-06

LATE = 256


def spread(array, axis):
    count = lax.axis_size(axis)
    copies = jnp.broadcast_to(array[None], (count,) + array.shape)
    return lax.all_to_all(copies, axis, 0, 0, tiled=True)


def down_kernel(core_ref, hidden_ref, weight_ref, out_ref):
    groups, rows, depth = weight_ref.shape
    weight = weight_ref[...].reshape(groups * rows, depth)
    out_ref[0] = lax.dot_general(
        hidden_ref[...], weight, (((1,), (1,)), ((), ())), preferred_element_type=jnp.float32
    ).astype(out_ref.dtype)


def down_blocks(core, hidden, gathered, rows, columns, blocks, dtype):
    tokens, depth = hidden.shape
    groups = columns // rows
    return pl.pallas_call(
        down_kernel,
        grid_spec=pltpu.PrefetchScalarGridSpec(
            num_scalar_prefetch=1,
            grid=(blocks,),
            in_specs=[
                pl.BlockSpec((tokens, depth), lambda i, core_ref: (0, 0)),
                pl.BlockSpec((groups, rows, depth), lambda i, core_ref: (2 * i + core_ref[0], 0, 0)),
            ],
            out_specs=pl.BlockSpec((1, tokens, columns), lambda i, core_ref: (i, 0, 0)),
        ),
        out_shape=jax.ShapeDtypeStruct((blocks, tokens, columns), dtype),
        cost_estimate=pl.CostEstimate(
            flops=2 * tokens * depth * columns * blocks,
            bytes_accessed=2 * (tokens * depth + columns * depth * blocks + tokens * columns * blocks),
            transcendentals=0,
        ),
    )(core.reshape(1), hidden, gathered)


def local(tokens, norm_gain, up_weight, up_scale, down_weight, down_scale):
    up_half = up_weight.astype(jnp.bfloat16)
    down_rows = (down_weight.T * down_scale[:, None]).astype(jnp.bfloat16)
    rows, hidden_width = up_half.shape
    early_width = hidden_width - LATE
    parts = hidden_width // LATE
    late_rows = rows // parts
    late = jnp.concatenate(
        [up_half[i * late_rows : (i + 1) * late_rows, early_width:] for i in range(parts)], axis=1
    )
    both = spread(jnp.concatenate([down_rows, late], axis=0), "y")
    early, both = lax.optimization_barrier((up_half[:, :early_width], both))
    gathered = lax.all_gather(both, "z", axis=0, tiled=True)
    early = lax.all_gather(early, "z", axis=0, tiled=False)
    early = spread(early, "y")
    early = early.transpose(1, 0, 2, 3).reshape(-1, early_width)

    floats = tokens.astype(jnp.float32)
    inverse = lax.rsqrt(jnp.mean(floats * floats, axis=-1, keepdims=True) + epsilon)
    normed = lax.optimization_barrier((floats * inverse * norm_gain).astype(jnp.bfloat16))

    def activated(weight, scale):
        pre = jnp.dot(normed, weight, preferred_element_type=jnp.float32) * scale
        return lax.optimization_barrier(jnp.square(jax.nn.relu(pre)).astype(jnp.bfloat16))

    early_hidden = activated(early, up_scale[:early_width])
    late_up = gathered[:, rows:].reshape(-1, late_rows, parts, LATE)
    late_up = late_up.transpose(0, 2, 1, 3).reshape(-1, LATE)
    late_hidden = activated(late_up, up_scale[early_width:])
    hidden = jnp.concatenate([early_hidden, late_hidden], axis=1)

    core = lax.axis_index("c")
    cores, chips = lax.axis_size("c"), lax.axis_size("x")
    columns = down_scale.shape[0] * lax.axis_size("z") * lax.axis_size("y") // (cores * chips)
    theirs = down_blocks(1 - core, hidden, gathered, rows, columns, chips, jnp.bfloat16)
    arrived = lax.ppermute(theirs, "c", [(0, 1), (1, 0)])
    mine = down_blocks(core, hidden, gathered, rows, columns, chips, jnp.float32)
    chip_sum = (mine + arrived.astype(jnp.float32)).astype(jnp.bfloat16)
    tiles = lax.all_to_all(chip_sum, "x", 0, 0, tiled=True).astype(jnp.float32)
    return ((tiles[0] + tiles[1]) + (tiles[2] + tiles[3])).astype(jnp.bfloat16)


def solution(mesh):
    split = Mesh(mesh.devices.reshape(16, 4, 4, 2), FS + TP)
    return jax.shard_map(
        local,
        mesh=split,
        in_specs=(P(FS, None), P(), P(FS, TP), P(TP), P(TP, FS), P(FS)),
        out_specs=P(FS, TP),
        check_vma=False,
    )
```

time: 362 us -> 162 us (0.45)
  waiting for transfers between devices: 277 us -> 32.3 us
  starting transfers between devices: 0.04 us -> 17.4 us
  blocking collectives: 51.1 us -> 63.4 us
  Pallas kernels: 0 us -> 11.2 us
  matrix products: 13 us -> 4.69 us
  local copies, waits for them, and re-layouts: 0.22 us -> 7.2 us
  other arithmetic: 7.15 us -> 12 us
    all_gather x2 -> x1, waiting for transfers between devices: 277 us -> 3.43 us  [local(): gathered = lax.all_gather(both, 'z', axis=0, tiled=True)]
    all_gather x0 -> x1, blocking collectives: none -> 38.6 us  [local(): early = lax.all_gather(early, 'z', axis=0, tiled=False)]
    all_to_all x0 -> x2, waiting for transfers between devices: none -> 28.8 us  [spread(): return lax.all_to_all(copies, axis, 0, 0, tiled=True)]
    all_to_all x1, blocking collectives: 51.1 us -> 24.8 us  [local(): tiles = lax.all_to_all(chip_sum, 'x', 0, 0, tiled=True).astype(jnp.float32)]
    pallas_call x0 -> x2, Pallas kernels: none -> 11.2 us  [down_blocks(): pl.pallas_call(down_kernel, grid_spec=pltpu.PrefetchScalarGridSpec(num_sc...]
    all_to_all x0 -> x2, starting transfers between devices: none -> 8.85 us  [spread(): return lax.all_to_all(copies, axis, 0, 0, tiled=True)]
    ppermute x0 -> x1, starting transfers between devices: none -> 8.6 us  [local(): arrived = lax.ppermute(theirs, 'c', [(0, 1), (1, 0)])]
    dot_general x2, matrix products: 13 us -> 4.69 us  [activated(): pre = jnp.dot(normed, weight, preferred_element_type=jnp.float32) * scale]
  transfers between devices with their start and end apart: 2 -> 4, of which waited for: 2 -> 3; matrix products, arithmetic and copies ran while one was open for 3% -> 7% of each run, Pallas kernels for 0% -> 4%
where the time goes in v2:
time: 162 us
  blocking collectives  63.4 us (39%)
  waiting for transfers between devices  32.3 us (20%)
  starting transfers between devices  17.4 us (11%)
  between operations  13.5 us (8%)
  other arithmetic  12 us (7%)
  Pallas kernels  11.2 us (7%)
  local copies, waits for them, and re-layouts  7.2 us (4%)
  matrix products  4.69 us (3%)
    all_gather x1, blocking collectives, local(): early = lax.all_gather(early, 'z', axis=0, tiled=False)  38.6 us
    all_to_all x2, waiting for transfers between devices, spread(): return lax.all_to_all(copies, axis, 0, 0, tiled=True)  28.8 us
    all_to_all x1, blocking collectives, local(): tiles = lax.all_to_all(chip_sum, 'x', 0, 0, tiled=True).astype(jnp.float32)  24.8 us
    pallas_call x2, Pallas kernels, down_blocks(): pl.pallas_call(down_kernel, grid_spec=pltpu.PrefetchScalarGridSpec(num_sc...  11.2 us
    all_to_all x2, starting transfers between devices, spread(): return lax.all_to_all(copies, axis, 0, 0, tiled=True)  8.85 us
    ppermute x1, starting transfers between devices, local(): arrived = lax.ppermute(theirs, 'c', [(0, 1), (1, 0)])  8.6 us
    dot_general x2, matrix products, activated(): pre = jnp.dot(normed, weight, preferred_element_type=jnp.float32) * scale  4.69 us
    all_gather x1, waiting for transfers between devices, local(): gathered = lax.all_gather(both, 'z', axis=0, tiled=True)  3.43 us
  transfers between devices with their start and end apart: 4, of which 3 were waited for; matrix products, arithmetic and copies ran while one was open for 7% of the time, Pallas kernels for 4%

profile of v2, /device:TPU:1, one launch (start us, length us, event | category | flops | bytes accessed | tf_op | source)
XLA Modules:
  0.0 161.7 jit_solution(13590675081255366924)
XLA Ops:
  6.5 0.9 convert_element_type.38
  7.5 1.0 fusion.9
  8.5 0.8 broadcast_in_dim.4
  9.2 5.0 %all-to-all-start = ((bf16[4,40,1024]{2,1,0:T(8,128)(2,1)}), bf16[4,40,1024]{2,1,0:T(8,128)(2,1)S(1)}, u32[]{:S(2)}, u32[]{:S(2)}) async-start(bf16[4,40,1024]{2,1,0:T(8,128)(2,1)} %broadcast_in_dim.4), calls=%async_computation | async-start | bytes 655360 | tf_op jit(solution)/shard_map/all_to_all | solution.py:20
  14.2 0.0 all-gather.3.cloned.1.call-start
  14.2 5.9 %all-to-all-done = bf16[4,40,1024]{2,1,0:T(8,128)(2,1)S(1)} async-done(((bf16[4,40,1024]{2,1,0:T(8,128)(2,1)}), bf16[4,40,1024]{2,1,0:T(8,128)(2,1)S(1)}, u32[]{:S(2)}, u32[]{:S(2)}) %all-to-all-start) | async-done | bytes 327712 | tf_op jit(solution)/shard_map/all_to_all | solution.py:20
  20.1 0.0 copy-start.3
  20.1 0.7 copy-done.3
  20.8 0.0 all-gather.3.cloned.1.call-update
  20.9 38.6 %all-gather = bf16[512,768]{1,0:T(8,128)(2,1)S(1)} all-gather(bf16[32,768]{1,0:T(8,128)(2,1)S(1)} %slice.48), channel_id=2, replica_groups=mesh['z'=16,'y'=4,'x'=4,'c'=2] {'z'}, dimensions={0}, use_global_device_ids=true | all-gather | bytes 835584 | tf_op jit(solution)/shard_map/all_gather | solution.py:67
  59.4 2.1 %broadcast_in_dim.5 = bf16[4,16,32,768]{3,2,1,0:T(8,128)(2,1)} broadcast(bf16[16,32,768]{2,1,0:T(8,128)(2,1)S(1)} %bitcast.21), dimensions={1,2,3} | broadcast | bytes 3932160 | tf_op jit(solution)/shard_map/broadcast_in_dim | solution.py:19
  61.5 0.0 copy-start.6
  61.5 3.8 %all-to-all-start.1 = ((bf16[4,16,32,768]{3,2,1,0:T(8,128)(2,1)}), bf16[4,16,32,768]{3,2,1,0:T(8,128)(2,1)S(1)}, u32[]{:S(2)}, u32[]{:S(2)}) async-start(bf16[4,16,32,768]{3,2,1,0:T(8,128)(2,1)} %broadcast_in_dim.5), calls=%async_computation.1 | async-start | bytes 6291456 | tf_op jit(solution)/shard_map/all_to_all | solution.py:20
  65.4 0.0 copy-start.5
  65.4 0.0 copy-done.6
  65.4 0.0 copy-start
  65.4 2.8 %fusion = f32[768]{0:T(1024)S(1)} fusion(bf16[768,2048]{1,0:T(8,128)(2,1)} %param.6), kind=kLoop, calls=%fused_computation.2 | loop fusion | flops 4717824 | bytes 3148800 | tf_op jit(solution)/shard_map/reduce_sum | solution.py:72
  68.2 0.0 copy-done.5
  68.2 0.1 copy-done
  68.3 2.4 %fusion.2 = bf16[768,2048]{1,0:T(8,128)(2,1)} fusion(bf16[768,2048]{1,0:T(8,128)(2,1)S(1)} %copy-done, f32[2048]{0:T(1024)S(1)} %copy-done.5, f32[768]{0:T(1024)S(1)} %add_rsqrt_fusion), kind=kLoop, calls=%fused_computation.4 | loop fusion | flops 6291456 | bytes 6302720 | tf_op jit(solution)/shard_map/convert_element_type | solution.py:73
  70.8 23.0 %all-to-all-done.1 = bf16[4,16,32,768]{3,2,1,0:T(8,128)(2,1)S(1)} async-done(((bf16[4,16,32,768]{3,2,1,0:T(8,128)(2,1)}), bf16[4,16,32,768]{3,2,1,0:T(8,128)(2,1)S(1)}, u32[]{:S(2)}, u32[]{:S(2)}) %all-to-all-start.1) | async-done | bytes 3145760 | tf_op jit(solution)/shard_map/all_to_all | solution.py:20
  93.7 0.0 copy-start.1
  93.7 0.3 copy.7
  94.0 1.6 %copy-done.1 = bf16[768,2048]{1,0:T(8,128)(2,1)S(1)} copy-done((bf16[768,2048]{1,0:T(8,128)(2,1)S(1)}, bf16[768,2048]{1,0:T(8,128)(2,1)}, u32[]{:S(2)}) %copy-start.1) | copy-done | bytes 3145752
  95.7 0.0 copy-start.2
  95.7 3.7 %multiply_convert_fusion = bf16[768,768]{1,0:T(8,128)(2,1)} fusion(bf16[768,2048]{1,0:T(8,128)(2,1)S(1)} %copy-done.1, bf16[2048,768]{1,0:T(8,128)(2,1)S(1)} %bitcast.20, f32[768]{0:T(1024)S(1)} %bitcast.23), kind=kOutput, calls=%fused_computation.6 | convolution fusion | flops 2418278400 | bytes 7474176 | tf_op jit(solution)/shard_map/dot_general | solution.py:76
  99.4 3.4 %all-gather.3.cloned.1.call-done.weight_ref = bf16[64,40,1024]{2,1,0:T(8,128)(2,1)} async-done(((bf16[4,40,1024]{2,1,0:T(8,128)(2,1)}), bf16[64,40,1024]{2,1,0:T(8,128)(2,1)}) %all-gather.3.cloned.1.call-update) | async-done | bytes 5242896 | tf_op jit(solution)/shard_map/all_gather | solution.py:66
  102.8 1.3 slice.53
  104.1 0.0 copy-done.2
  104.1 0.0 copy-start.4
  104.1 1.0 fusion.5
  105.1 0.3 copy-done.4
  105.4 1.4 pad_maximum_fusion.hidden_ref
  106.8 5.4 %shard_map.65 = bf16[4,768,256]{2,1,0:T(8,128)(2,1)} custom-call(s32[1]{0:T(128)} %bitcast.8.core_ref, bf16[768,1024]{1,0:T(8,128)(2,1)} %pad_maximum_fusion.hidden_ref, bf16[64,40,1024]{2,1,0:T(8,128)(2,1)} %all-gather.3.cloned.1.call-done.weight_ref), custom_call_target="tpu_custom_call" | custom-call | flops 1610612736 | bytes 5242880 | tf_op jit(solution)/shard_map/pallas_call | solution.py:34
  112.2 8.6 %collective-permute-start = (bf16[4,768,256]{2,1,0:T(8,128)(2,1)}, bf16[4,768,256]{2,1,0:T(8,128)(2,1)S(1)}, u32[]{:S(2)}, u32[]{:S(2)}) collective-permute-start(bf16[4,768,256]{2,1,0:T(8,128)(2,1)} %shard_map.65), channel_id=1, source_target_pairs={{0,1},{1,0},{2,3},{3,2},{4,5},{5,4},{6,7},{7,6},{8,9},{9,8},{10,11... | collective-permute-start | bytes 4718600 | tf_op jit(solution)/shard_map/ppermute | solution.py:89
  120.8 5.8 %shard_map.64 = f32[4,768,256]{2,1,0:T(8,128)} custom-call(s32[1]{0:T(128)} %bitcast.core_ref, bf16[768,1024]{1,0:T(8,128)(2,1)} %pad_maximum_fusion.hidden_ref, bf16[64,40,1024]{2,1,0:T(8,128)(2,1)} %all-gather.3.cloned.1.call-done.weight_ref), custom_call_target="tpu_custom_call" | custom-call | flops 1610612736 | bytes 5242880 | tf_op jit(solution)/shard_map/pallas_call | solution.py:34
  126.6 0.0 collective-permute-done
  126.6 2.3 %add_convert_fusion = bf16[4,768,256]{2,1,0:T(8,128)(2,1)S(1)} fusion(f32[4,768,256]{2,1,0:T(8,128)} %shard_map.64, bf16[4,768,256]{2,1,0:T(8,128)(2,1)S(1)} %collective-permute-done), kind=kLoop, calls=%fused_computation.5 | loop fusion | flops 2359296 | bytes 6291456 | tf_op jit(solution)/shard_map/convert_element_type | solution.py:91
  128.8 24.8 %all_to_all.15 = bf16[4,768,256]{2,1,0:T(8,128)(2,1)S(1)} all-to-all(bf16[4,768,256]{2,1,0:T(8,128)(2,1)S(1)} %add_convert_fusion), channel_id=1, replica_groups=mesh['z'=16,'y'=4,'x'=4,'c'=2] {'x'}, dimensions={0} | all-to-all | bytes 3145728 | tf_op jit(solution)/shard_map/all_to_all | solution.py:92
  153.6 0.3 convert_element_type.45
  153.9 0.9 fusion.8
  (5 shorter events, 0.0 us)
Async XLA Ops:
  9.2 10.9 %all-to-all-start = ((bf16[4,40,1024]{2,1,0:T(8,128)(2,1)}), bf16[4,40,1024]{2,1,0:T(8,128)(2,1)S(1)}, u32[]{:S(2)}, u32[]{:S(2)}) async-start(bf16[4,40,1024]{2,1,0:T(8,128)(2,1)} %broadcast_in_dim.4), calls=%async_computation | async-start | bytes 655360 | tf_op jit(solution)/shard_map/all_to_all | solution.py:20
  14.2 88.6 %all-gather.3.cloned.1.call-start = ((), (), s32[]{:S(2)}) async-start(), calls=%async_computation.3 | async-start | bytes 5570560 | tf_op jit(solution)/shard_map/all_gather | solution.py:66
  20.1 0.7 copy-start.3
  61.5 3.9 %copy-start.6 = (f32[1024]{0:T(1024)S(1)}, f32[1024]{0:T(1024)}, u32[]{:S(2)}) copy-start(f32[1024]{0:T(1024)} %param.9) | copy-start | bytes 12292
  61.5 32.2 %all-to-all-start.1 = ((bf16[4,16,32,768]{3,2,1,0:T(8,128)(2,1)}), bf16[4,16,32,768]{3,2,1,0:T(8,128)(2,1)S(1)}, u32[]{:S(2)}, u32[]{:S(2)}) async-start(bf16[4,16,32,768]{3,2,1,0:T(8,128)(2,1)} %broadcast_in_dim.5), calls=%async_computation.1 | async-start | bytes 6291456 | tf_op jit(solution)/shard_map/all_to_all | solution.py:20
  65.4 2.8 %copy-start.5 = (f32[2048]{0:T(1024)S(1)}, f32[2048]{0:T(1024)}, u32[]{:S(2)}) copy-start(f32[2048]{0:T(1024)} %param.7) | copy-start | bytes 24580
  65.4 2.9 %copy-start = (bf16[768,2048]{1,0:T(8,128)(2,1)S(1)}, bf16[768,2048]{1,0:T(8,128)(2,1)}, u32[]{:S(2)}) copy-start(bf16[768,2048]{1,0:T(8,128)(2,1)} %param.6) | copy-start | bytes 9437188
  93.7 1.9 %copy-start.1 = (bf16[768,2048]{1,0:T(8,128)(2,1)S(1)}, bf16[768,2048]{1,0:T(8,128)(2,1)}, u32[]{:S(2)}) copy-start(bf16[768,2048]{1,0:T(8,128)(2,1)} %fusion.2) | copy-start | bytes 9437188
  95.7 8.4 %copy-start.2 = (bf16[768,2048]{1,0:T(8,128)(2,1)S(1)}, bf16[768,2048]{1,0:T(8,128)(2,1)}, u32[]{:S(2)}) copy-start(bf16[768,2048]{1,0:T(8,128)(2,1)} %fusion.2) | copy-start | bytes 9437188
  104.1 1.3 copy-start.4
  112.2 14.4 %collective-permute-start = (bf16[4,768,256]{2,1,0:T(8,128)(2,1)}, bf16[4,768,256]{2,1,0:T(8,128)(2,1)S(1)}, u32[]{:S(2)}, u32[]{:S(2)}) collective-permute-start(bf16[4,768,256]{2,1,0:T(8,128)(2,1)} %shard_map.65), channel_id=1, source_target_pairs={{0,1},{1,0},{2,3},{3,2},{4,5},{5,4},{6,7},{7,6},{8,9},{9,8},{10,11... | collective-permute-start | bytes 4718600 | tf_op jit(solution)/shard_map/ppermute | solution.py:89
Sparse Core Ops, SparseCore 0:
  21.0 81.7 all-gather.2

commit v3 on v2

v3 whole, which is shorter than its diff:
```python
import jax
import jax.numpy as jnp
from jax import lax
from jax.experimental import pallas as pl
from jax.experimental.pallas import tpu as pltpu
from jax.sharding import Mesh
from jax.sharding import PartitionSpec as P

FS = ("z", "y")
TP = ("x", "c")

epsilon = 1e-06

LATE = 256


def spread(array, axis):
    count = lax.axis_size(axis)
    copies = jnp.broadcast_to(array[None], (count,) + array.shape)
    return lax.all_to_all(copies, axis, 0, 0, tiled=True)


def prepare_kernel(up_ref, down_ref, scale_ref, copies_ref, early_ref):
    rows, width = down_ref.shape
    early_width = early_ref.shape[1]
    late_width = width - early_width
    late_rows = copies_ref.shape[1] - rows
    at = lax.broadcasted_iota(jnp.int32, (rows, rows), 0)
    to = lax.broadcasted_iota(jnp.int32, (rows, rows), 1)
    scale = jnp.sum(jnp.where(at == to, scale_ref[...], 0.0), axis=1, keepdims=True)
    down = (down_ref[...] * scale).astype(jnp.bfloat16)
    early_ref[...] = up_ref[:, :early_width].astype(jnp.bfloat16)
    for k in range(copies_ref.shape[0]):
        copies_ref[k, :rows, :] = down
        for i in range(rows // late_rows):
            copies_ref[k, rows:, i * late_width : (i + 1) * late_width] = up_ref[
                i * late_rows : (i + 1) * late_rows, early_width:
            ].astype(jnp.bfloat16)


def down_kernel(core_ref, early_ref, late_ref, gathered_ref, out_ref):
    blocks, _, columns = out_ref.shape
    early_width = early_ref.shape[1]
    depth = gathered_ref.shape[2]
    groups = gathered_ref.shape[0] // (2 * blocks)
    rows = columns // groups
    contract = (((1,), (1,)), ((), ()))
    for i in range(blocks):
        first = (2 * i + core_ref[0]) * groups
        weight = gathered_ref[pl.ds(first, groups), 0:rows, :].reshape(columns, depth)
        total = lax.dot_general(
            early_ref[...], weight[:, :early_width], contract, preferred_element_type=jnp.float32
        ) + lax.dot_general(
            late_ref[...], weight[:, early_width:], contract, preferred_element_type=jnp.float32
        )
        out_ref[i] = total.astype(out_ref.dtype)


def down_blocks(core, early, late, gathered, columns, blocks, dtype):
    tokens = early.shape[0]
    depth = early.shape[1] + late.shape[1]
    vmem = pl.BlockSpec(memory_space=pltpu.VMEM)
    return pl.pallas_call(
        down_kernel,
        in_specs=[pl.BlockSpec(memory_space=pltpu.SMEM), vmem, vmem, vmem],
        out_specs=vmem,
        out_shape=jax.ShapeDtypeStruct((blocks, tokens, columns), dtype),
        cost_estimate=pl.CostEstimate(
            flops=2 * tokens * depth * columns * blocks,
            bytes_accessed=2 * (tokens * depth + columns * depth * blocks + tokens * columns * blocks),
            transcendentals=0,
        ),
        compiler_params=pltpu.CompilerParams(vmem_limit_bytes=24 * 2**20),
    )(core.reshape(1), early, late, gathered)


def local(tokens, norm_gain, up_weight, up_scale, down_weight, down_scale):
    rows, hidden_width = up_weight.shape
    early_width = hidden_width - LATE
    parts = hidden_width // LATE
    late_rows = rows // parts
    vmem = pl.BlockSpec(memory_space=pltpu.VMEM)
    copies, early = pl.pallas_call(
        prepare_kernel,
        in_specs=[vmem, vmem, vmem],
        out_specs=[vmem, vmem],
        out_shape=[
            jax.ShapeDtypeStruct(
                (lax.axis_size("y"), rows + late_rows, hidden_width), jnp.bfloat16
            ),
            jax.ShapeDtypeStruct((rows, early_width), jnp.bfloat16),
        ],
    )(up_weight, down_weight.T, down_scale.reshape(1, rows))
    both = lax.all_to_all(copies, "y", 0, 0, tiled=True)
    early, both = lax.optimization_barrier((early, both))
    gathered = lax.all_gather(both, "z", axis=0, tiled=True)
    early = lax.all_gather(early, "z", axis=0, tiled=False)
    early = spread(early, "y")
    early = early.transpose(1, 0, 2, 3).reshape(-1, early_width)

    floats = tokens.astype(jnp.float32)
    inverse = lax.rsqrt(jnp.mean(floats * floats, axis=-1, keepdims=True) + epsilon)
    normed = lax.optimization_barrier((floats * inverse * norm_gain).astype(jnp.bfloat16))

    def activated(weight, scale):
        pre = jnp.dot(normed, weight, preferred_element_type=jnp.float32) * scale
        return lax.optimization_barrier(jnp.square(jax.nn.relu(pre)).astype(jnp.bfloat16))

    early_hidden = activated(early, up_scale[:early_width])
    late_up = gathered[:, rows:].reshape(-1, late_rows, parts, LATE)
    late_up = late_up.transpose(0, 2, 1, 3).reshape(-1, LATE)
    late_hidden = activated(late_up, up_scale[early_width:])
    core = lax.axis_index("c")
    cores, chips = lax.axis_size("c"), lax.axis_size("x")
    columns = down_scale.shape[0] * lax.axis_size("z") * lax.axis_size("y") // (cores * chips)
    theirs = down_blocks(1 - core, early_hidden, late_hidden, gathered, columns, chips, jnp.bfloat16)
    arrived = lax.ppermute(theirs, "c", [(0, 1), (1, 0)])
    mine = down_blocks(core, early_hidden, late_hidden, gathered, columns, chips, jnp.float32)
    chip_sum = (mine + arrived.astype(jnp.float32)).astype(jnp.bfloat16)
    tiles = lax.all_to_all(chip_sum, "x", 0, 0, tiled=True).astype(jnp.float32)
    return ((tiles[0] + tiles[1]) + (tiles[2] + tiles[3])).astype(jnp.bfloat16)


def solution(mesh):
    split = Mesh(mesh.devices.reshape(16, 4, 4, 2), FS + TP)
    return jax.shard_map(
        local,
        mesh=split,
        in_specs=(P(FS, None), P(), P(FS, TP), P(TP), P(TP, FS), P(FS)),
        out_specs=P(FS, TP),
        check_vma=False,
    )
```

time: 162 us -> 152 us (0.938)
  blocking collectives: 63.4 us -> 73.7 us
  Pallas kernels: 11.2 us -> 5.44 us
  other arithmetic: 12 us -> 6.89 us
  starting transfers between devices: 17.4 us -> 12.4 us
  waiting for transfers between devices: 32.3 us -> 28.3 us
  local copies, waits for them, and re-layouts: 7.2 us -> 5.57 us
    all_to_all x0 -> x1, blocking collectives: none -> 11 us  [local(): both = lax.all_to_all(copies, 'y', 0, 0, tiled=True)]
    all_to_all x2 -> x1, waiting for transfers between devices: 28.8 us -> 22.7 us  [spread(): return lax.all_to_all(copies, axis, 0, 0, tiled=True)]
    pallas_call x2 -> x3, Pallas kernels: 11.2 us -> 5.44 us  [the longest x2 3.65 us: down_blocks(): pl.pallas_call(down_kernel, in_specs=[pl.BlockSpec(memory_space=pltpu.SME...]
    all_to_all x2 -> x1, starting transfers between devices: 8.85 us -> 3.7 us  [spread(): return lax.all_to_all(copies, axis, 0, 0, tiled=True)]
    convert_element_type x2 -> x0, other arithmetic: 1.9 us -> none  [the longest x1 0.99 us: local(): down_rows = (down_weight.T * down_scale[:, None]).astype(jnp.bfloat16)]
    convert_element_type x1, other arithmetic: 2.26 us -> 0.51 us  [local(): chip_sum = (mine + arrived.astype(jnp.float32)).astype(jnp.bfloat16)]
  transfers between devices with their start and end apart: 4 -> 3, of which waited for: 3 -> 3; matrix products, arithmetic and copies ran while one was open for 7% -> 7% of each run, Pallas kernels for 4% -> 1%
where the time goes in v3:
time: 152 us; the launch traced here: 151 us
  blocking collectives  73.7 us (48%)
  waiting for transfers between devices  28.3 us (19%)
  between operations  13.5 us (9%)
  starting transfers between devices  12.4 us (8%)
  other arithmetic  6.89 us (5%)
  matrix products  5.61 us (4%)
  local copies, waits for them, and re-layouts  5.57 us (4%)
  Pallas kernels  5.44 us (4%)
    all_gather x1, blocking collectives, local(): early = lax.all_gather(early, 'z', axis=0, tiled=False)  39.1 us
    all_to_all x1, blocking collectives, local(): tiles = lax.all_to_all(chip_sum, 'x', 0, 0, tiled=True).astype(jnp.float32)  23.6 us
    all_to_all x1, waiting for transfers between devices, spread(): return lax.all_to_all(copies, axis, 0, 0, tiled=True)  22.7 us
    all_to_all x1, blocking collectives, local(): both = lax.all_to_all(copies, 'y', 0, 0, tiled=True)  11 us
    ppermute x1, starting transfers between devices, local(): arrived = lax.ppermute(theirs, 'c', [(0, 1), (1, 0)])  8.72 us
    dot_general x2, matrix products, activated(): pre = jnp.dot(normed, weight, preferred_element_type=jnp.float32) * scale  5.61 us
    all_gather x1, waiting for transfers between devices, local(): gathered = lax.all_gather(both, 'z', axis=0, tiled=True)  4.4 us
    all_to_all x1, starting transfers between devices, spread(): return lax.all_to_all(copies, axis, 0, 0, tiled=True)  3.7 us
  transfers between devices with their start and end apart: 3, of which 3 were waited for; matrix products, arithmetic and copies ran while one was open for 7% of the time, Pallas kernels for 1%

profile of v3, /device:TPU:1, one launch (start us, length us, event | category | flops | bytes accessed | tf_op | source)
XLA Modules:
  0.0 151.5 jit_solution(9656611040513924783)
XLA Ops:
  6.5 0.0 all-gather.3.cloned.1.call-start
  6.5 1.8 %shard_map.64 = (bf16[4,40,1024]{2,1,0:T(8,128)(2,1)}, bf16[32,768]{1,0:T(8,128)(2,1)}) custom-call(f32[32,1024]{1,0:T(8,128)} %up_ref.1, f32[32,1024]{1,0:T(8,128)} %bitcast.25, f32[1,32]{1,0:T(1,128)} %bitcast.26), custom_call_target="tpu_custom_call" | custom-call | tf_op jit(solution)/shard_map/pallas_call | solution.py:83
  8.3 11.0 %all_to_all.15 = bf16[4,40,1024]{2,1,0:T(8,128)(2,1)} all-to-all(bf16[4,40,1024]{2,1,0:T(8,128)(2,1)} %get-tuple-element.10), channel_id=1, replica_groups=mesh['z'=16,'y'=4,'x'=4,'c'=2] {'y'}, dimensions={0} | all-to-all | bytes 655360 | tf_op jit(solution)/shard_map/all_to_all | solution.py:94
  19.3 0.0 all-gather.3.cloned.1.call-update
  19.3 39.1 %all-gather = bf16[512,768]{1,0:T(8,128)(2,1)S(1)} all-gather(bf16[32,768]{1,0:T(8,128)(2,1)} %get-tuple-element.11), channel_id=2, replica_groups=mesh['z'=16,'y'=4,'x'=4,'c'=2] {'z'}, dimensions={0}, use_global_device_ids=true | all-gather | bytes 835584 | tf_op jit(solution)/shard_map/all_gather | solution.py:97
  58.4 2.1 %broadcast_in_dim.2 = bf16[4,16,32,768]{3,2,1,0:T(8,128)(2,1)} broadcast(bf16[16,32,768]{2,1,0:T(8,128)(2,1)S(1)} %bitcast.23), dimensions={1,2,3} | broadcast | bytes 3932160 | tf_op jit(solution)/shard_map/broadcast_in_dim | solution.py:19
  60.5 3.7 %all-to-all-start.1 = ((bf16[4,16,32,768]{3,2,1,0:T(8,128)(2,1)}), bf16[4,16,32,768]{3,2,1,0:T(8,128)(2,1)S(1)}, u32[]{:S(2)}, u32[]{:S(2)}) async-start(bf16[4,16,32,768]{3,2,1,0:T(8,128)(2,1)} %broadcast_in_dim.2), calls=%async_computation.1 | async-start | bytes 6291456 | tf_op jit(solution)/shard_map/all_to_all | solution.py:20
  64.3 0.0 copy-start.2
  64.3 0.0 copy-start
  64.3 2.7 %fusion = f32[768]{0:T(1024)S(1)} fusion(bf16[768,2048]{1,0:T(8,128)(2,1)} %param.6), kind=kLoop, calls=%fused_computation.2 | loop fusion | flops 4717824 | bytes 3148800 | tf_op jit(solution)/shard_map/reduce_sum | solution.py:102
  67.0 0.0 copy-done.2
  67.1 0.1 copy-done
  67.1 0.0 copy-start.3
  67.1 2.4 %fusion.2 = bf16[768,2048]{1,0:T(8,128)(2,1)} fusion(bf16[768,2048]{1,0:T(8,128)(2,1)S(1)} %copy-done, f32[2048]{0:T(1024)S(1)} %copy-done.2, f32[768]{0:T(1024)S(1)} %add_rsqrt_fusion), kind=kLoop, calls=%fused_computation.4 | loop fusion | flops 6291456 | bytes 6302720 | tf_op jit(solution)/shard_map/convert_element_type | solution.py:103
  69.6 0.0 copy-done.3
  69.6 22.7 %all-to-all-done.1 = bf16[4,16,32,768]{3,2,1,0:T(8,128)(2,1)S(1)} async-done(((bf16[4,16,32,768]{3,2,1,0:T(8,128)(2,1)}), bf16[4,16,32,768]{3,2,1,0:T(8,128)(2,1)S(1)}, u32[]{:S(2)}, u32[]{:S(2)}) %all-to-all-start.1) | async-done | bytes 3145760 | tf_op jit(solution)/shard_map/all_to_all | solution.py:20
  92.3 0.0 copy-start.1
  92.3 0.3 copy.7
  92.6 1.6 %copy-done.1 = bf16[768,2048]{1,0:T(8,128)(2,1)S(1)} copy-done((bf16[768,2048]{1,0:T(8,128)(2,1)S(1)}, bf16[768,2048]{1,0:T(8,128)(2,1)}, u32[]{:S(2)}) %copy-start.1) | copy-done | bytes 3145752
  94.2 2.6 %multiply_convert_fusion.early_ref = bf16[768,768]{1,0:T(8,128)(2,1)S(1)} fusion(bf16[768,2048]{1,0:T(8,128)(2,1)S(1)} %copy-done.1, bf16[2048,768]{1,0:T(8,128)(2,1)S(1)} %bitcast.22, f32[768]{0:T(1024)S(1)} %bitcast.27), kind=kOutput, calls=%fused_computation.6 | convolution fusion | flops 2418278400 | bytes 7474176 | tf_op jit(solution)/shard_map/dot_general | solution.py:106
  96.8 4.4 %all-gather.3.cloned.1.call-done.gathered_ref = bf16[64,40,1024]{2,1,0:T(8,128)(2,1)} async-done(((bf16[4,40,1024]{2,1,0:T(8,128)(2,1)}), bf16[64,40,1024]{2,1,0:T(8,128)(2,1)}) %all-gather.3.cloned.1.call-update) | async-done | bytes 5242896 | tf_op jit(solution)/shard_map/all_gather | solution.py:96
  101.2 0.0 slice-start
  101.3 1.4 slice.28
  102.7 0.0 slice-start.1
  102.7 3.0 %fusion.5.late_ref = bf16[768,256]{1,0:T(8,128)(2,1)S(1)} fusion(bf16[768,2048]{1,0:T(8,128)(2,1)} %fusion.2, bf16[2048,256]{1,0:T(8,128)(2,1)S(1)} %bitcast.24, f32[256]{0:T(256)S(1)} %slice.23), kind=kOutput, calls=%fused_computation.10 | convolution fusion | flops 806092800 | bytes 4588544 | tf_op jit(solution)/shard_map/dot_general | solution.py:106
  105.7 0.0 slice-done
  105.7 0.0 slice-done.1
  105.8 1.8 %shard_map.66 = bf16[4,768,256]{2,1,0:T(8,128)(2,1)S(1)} custom-call(s32[1]{0:T(128)} %bitcast.9.core_ref, bf16[768,768]{1,0:T(8,128)(2,1)S(1)} %multiply_convert_fusion.early_ref, bf16[768,256]{1,0:T(8,128)(2,1)S(1)} %fusion.5.late_ref, bf16[64,40,1024]{2,1,0:T(8,128)(2,1)S(1)} %bitcast.21), custom_call_target="tpu_custom_call" | custom-call | flops 1610612736 | bytes 5242880 | tf_op jit(solution)/shard_map/pallas_call | solution.py:63
  107.6 8.7 %collective-permute-start = (bf16[4,768,256]{2,1,0:T(8,128)(2,1)S(1)}, bf16[4,768,256]{2,1,0:T(8,128)(2,1)S(1)}, u32[]{:S(2)}, u32[]{:S(2)}) collective-permute-start(bf16[4,768,256]{2,1,0:T(8,128)(2,1)S(1)} %shard_map.66), channel_id=1, source_target_pairs={{0,1},{1,0},{2,3},{3,2},{4,5},{5,4},{6,7},{7,6},{8,9},{9,8},{10,11... | collective-permute-start | bytes 4718600 | tf_op jit(solution)/shard_map/ppermute | solution.py:117
  116.3 1.8 %shard_map.65 = f32[4,768,256]{2,1,0:T(8,128)S(1)} custom-call(s32[1]{0:T(128)} %bitcast.core_ref, bf16[768,768]{1,0:T(8,128)(2,1)S(1)} %multiply_convert_fusion.early_ref, bf16[768,256]{1,0:T(8,128)(2,1)S(1)} %fusion.5.late_ref, bf16[64,40,1024]{2,1,0:T(8,128)(2,1)S(1)} %bitcast.21), custom_call_target="tpu_custom_call" | custom-call | flops 1610612736 | bytes 5242880 | tf_op jit(solution)/shard_map/pallas_call | solution.py:63
  118.2 1.2 collective-permute-done
  119.3 0.5 add_convert_fusion
  119.8 23.6 %all_to_all.16 = bf16[4,768,256]{2,1,0:T(8,128)(2,1)S(1)} all-to-all(bf16[4,768,256]{2,1,0:T(8,128)(2,1)S(1)} %add_convert_fusion), channel_id=1, replica_groups=mesh['z'=16,'y'=4,'x'=4,'c'=2] {'x'}, dimensions={0} | all-to-all | bytes 3145728 | tf_op jit(solution)/shard_map/all_to_all | solution.py:120
  143.4 0.3 convert_element_type.33
  143.7 0.9 fusion.8
  (3 shorter events, 0.0 us)
Async XLA Ops:
  6.5 94.7 %all-gather.3.cloned.1.call-start = ((), (), s32[]{:S(2)}) async-start(), calls=%async_computation.3 | async-start | bytes 5570560 | tf_op jit(solution)/shard_map/all_gather | solution.py:96
  60.5 31.8 %all-to-all-start.1 = ((bf16[4,16,32,768]{3,2,1,0:T(8,128)(2,1)}), bf16[4,16,32,768]{3,2,1,0:T(8,128)(2,1)S(1)}, u32[]{:S(2)}, u32[]{:S(2)}) async-start(bf16[4,16,32,768]{3,2,1,0:T(8,128)(2,1)} %broadcast_in_dim.2), calls=%async_computation.1 | async-start | bytes 6291456 | tf_op jit(solution)/shard_map/all_to_all | solution.py:20
  64.3 2.8 %copy-start.2 = (f32[2048]{0:T(1024)S(1)}, f32[2048]{0:T(1024)}, u32[]{:S(2)}) copy-start(f32[2048]{0:T(1024)} %param.7) | copy-start | bytes 24580
  64.3 2.9 %copy-start = (bf16[768,2048]{1,0:T(8,128)(2,1)S(1)}, bf16[768,2048]{1,0:T(8,128)(2,1)}, u32[]{:S(2)}) copy-start(bf16[768,2048]{1,0:T(8,128)(2,1)} %param.6) | copy-start | bytes 9437188
  67.1 2.4 %copy-start.3 = (f32[1024]{0:T(1024)S(1)}, f32[1024]{0:T(1024)}, u32[]{:S(2)}) copy-start(f32[1024]{0:T(1024)} %param.9) | copy-start | bytes 12292
  92.3 1.9 %copy-start.1 = (bf16[768,2048]{1,0:T(8,128)(2,1)S(1)}, bf16[768,2048]{1,0:T(8,128)(2,1)}, u32[]{:S(2)}) copy-start(bf16[768,2048]{1,0:T(8,128)(2,1)} %fusion.2) | copy-start | bytes 9437188
  101.2 4.5 %slice-start = ((s8[5242880]{0:T(1024)(128)(4,1)}), s8[4194304]{0:T(1024)(128)(4,1)S(1)}, s32[]{:S(2)}) async-start(s8[5242880]{0:T(1024)(128)(4,1)} %bitcast.20), calls=%async_computation.4 | async-start | bytes 8388608
  102.7 3.0 %slice-start.1 = ((s8[5242880]{0:T(1024)(128)(4,1)}), s8[1048576]{0:T(1024)(128)(4,1)S(1)}, s32[]{:S(2)}) async-start(s8[5242880]{0:T(1024)(128)(4,1)} %bitcast.20), calls=%async_computation.5 | async-start | bytes 2097152
  107.6 11.7 %collective-permute-start = (bf16[4,768,256]{2,1,0:T(8,128)(2,1)S(1)}, bf16[4,768,256]{2,1,0:T(8,128)(2,1)S(1)}, u32[]{:S(2)}, u32[]{:S(2)}) collective-permute-start(bf16[4,768,256]{2,1,0:T(8,128)(2,1)S(1)} %shard_map.66), channel_id=1, source_target_pairs={{0,1},{1,0},{2,3},{3,2},{4,5},{5,4},{6,7},{7,6},{8,9},{9,8},{10,11... | collective-permute-start | bytes 4718600 | tf_op jit(solution)/shard_map/ppermute | solution.py:117
Sparse Core Ops, SparseCore 0:
  19.5 81.7 all-gather.2
